TPU v7x, 32 devices: a whole 2x2x4 slice. The times are simulated.
32 devices in a mesh: sp: 8 (over z, y), dp: 4 (over x, core).
Axes of the slice: x: 2, y: 2, z: 4, core: 2. Of those that a mesh axis runs over, the one named last changes fastest.
Arguments:
- hidden_states: bfloat16 [8, 1024, 2048], P('dp', 'sp'), may hold values from -288 to 288
- cumulative_gate: float32 [8, 1024, 32], P('dp', 'sp'), may hold values from -4096 to 0, as said below
- query_weight: bfloat16 [2048, 2048], P('dp'), may hold values from -0.125 to 0.125
- key_weight: bfloat16 [2048, 512], P('dp'), may hold values from -0.125 to 0.125
- value_weight: bfloat16 [2048, 512], P('dp'), may hold values from -0.125 to 0.125
- out_weight: bfloat16 [2048, 2048], P('dp'), may hold values from -0.75 to 0.75
Outputs:
- mixed: bfloat16 [8, 1024, 2048], P('dp', 'sp')
Inputs may be any that keep to these rules, and one draw needn't show every extreme that they name: cumulative_gate never rises along a sequence and is at most 0.
All inputs are finite; a program needn't handle non-finite values.
Results may differ from a plain program's by a relative error of at most 0.009.
The roundings to bfloat16 on the way count: a program that leaves them out, or rounds other values in their place, can miss the bound.
Values may be sent and summed in bfloat16 or wider, within the bound.
A program may use at most 64 MiB of HBM per device.

v0:
```python
import math

import jax
import jax.numpy as jnp
from jax import lax
from jax.sharding import PartitionSpec as P

KV_HEADS = 8
HEAD = 64


def attend_one(query_head, key_head, value_head, gate_head):
    length = query_head.shape[0]
    block_rows = math.gcd(length, 512)
    block_count = length // block_rows
    key_index = jnp.arange(length, dtype=jnp.int32)
    scaling = query_head.shape[1] ** (-0.5)

    def one_block(block_number):
        offset = block_number * block_rows
        query_block = lax.dynamic_slice_in_dim(query_head, offset, block_rows, 0)
        gate_block = lax.dynamic_slice_in_dim(gate_head, offset, block_rows, 0)
        scores = jnp.dot(query_block, key_head.T, preferred_element_type=jnp.float32) * scaling
        scores = scores + gate_block[:, None] - gate_head[None, :]
        row_index = offset + jnp.arange(block_rows, dtype=jnp.int32)
        allowed = key_index[None, :] <= row_index[:, None]
        scores = jnp.where(allowed, scores, -jnp.inf)
        maximum = jnp.max(scores, axis=1, keepdims=True)
        exponent = jnp.where(allowed, jnp.exp(scores - maximum), 0.0)
        weights = (exponent / jnp.sum(exponent, axis=1, keepdims=True)).astype(jnp.bfloat16)
        return jnp.dot(weights, value_head, preferred_element_type=jnp.float32).astype(jnp.bfloat16)

    result = lax.map(one_block, jnp.arange(block_count, dtype=jnp.int32))
    return result.reshape(length, query_head.shape[1])


def on_device(hidden_states, cumulative_gate, query_weight, key_weight, value_weight, out_weight):
    sequences, positions, model_width = hidden_states.shape
    token_rows = hidden_states.reshape(sequences * positions, model_width)
    width_query = query_weight.shape[1]
    copies = max(1, lax.axis_size("sp") // KV_HEADS)

    def absorb(portion):
        return jnp.dot(token_rows, portion, preferred_element_type=jnp.float32)

    def spread(matrix):
        matrix = matrix.astype(jnp.bfloat16).reshape(sequences, positions, KV_HEADS, HEAD)
        return jnp.repeat(matrix, copies, axis=2).reshape(
            sequences, positions, KV_HEADS * copies * HEAD
        )

    summed = absorb(lax.all_gather(query_weight, "dp", axis=0, tiled=True))
    query_local = summed.astype(jnp.bfloat16).reshape(sequences, positions, width_query)
    key_sum = absorb(lax.all_gather(key_weight, "dp", axis=0, tiled=True))
    value_sum = absorb(lax.all_gather(value_weight, "dp", axis=0, tiled=True))
    key_local = spread(key_sum)
    value_local = spread(value_sum)
    query, key, value = (
        lax.all_to_all(query_local, "sp", split_axis=2, concat_axis=1, tiled=True),
        lax.all_to_all(key_local, "sp", split_axis=2, concat_axis=1, tiled=True),
        lax.all_to_all(value_local, "sp", split_axis=2, concat_axis=1, tiled=True),
    )
    gates = lax.all_to_all(cumulative_gate, "sp", split_axis=2, concat_axis=1, tiled=True)
    length = query.shape[1]
    heads_here = query.shape[2] // HEAD
    pairs_here = key.shape[2] // HEAD
    per_group = heads_here // pairs_here
    head_query = query.reshape(sequences, length, pairs_here, per_group, HEAD)
    head_query = jnp.transpose(head_query, (0, 2, 3, 1, 4)).reshape(
        sequences * pairs_here, per_group, length, HEAD
    )
    head_key = jnp.transpose(
        key.reshape(sequences, length, pairs_here, HEAD), (0, 2, 1, 3)
    ).reshape(sequences * pairs_here, length, HEAD)
    head_value = jnp.transpose(
        value.reshape(sequences, length, pairs_here, HEAD), (0, 2, 1, 3)
    ).reshape(sequences * pairs_here, length, HEAD)
    head_gate = jnp.transpose(
        gates.reshape(sequences, length, pairs_here, per_group), (0, 2, 3, 1)
    ).reshape(sequences * pairs_here, per_group, length)

    def per_pair(inputs):
        group_query, group_key, group_value, group_gate = inputs

        def per_head(head_inputs):
            return attend_one(head_inputs[0], group_key, group_value, head_inputs[1])

        return lax.map(per_head, (group_query, group_gate))

    attended = lax.map(per_pair, (head_query, head_key, head_value, head_gate))
    attended = attended.reshape(sequences, pairs_here, per_group, length, HEAD)
    attended = jnp.transpose(attended, (0, 3, 1, 2, 4)).reshape(
        sequences, length, heads_here * HEAD
    )
    returned = lax.all_to_all(attended, "sp", split_axis=1, concat_axis=2, tiled=True)
    returned_rows = returned.reshape(sequences * positions, width_query)
    mixed = jnp.dot(
        returned_rows,
        lax.all_gather(out_weight, "dp", axis=0, tiled=True),
        preferred_element_type=jnp.float32,
    )
    return mixed.astype(jnp.bfloat16).reshape(sequences, positions, model_width)


def solution(mesh):
    placed = (
        P("dp", "sp", None),
        P("dp", "sp", None),
        P("dp", None),
        P("dp", None),
        P("dp", None),
        P("dp", None),
    )
    return jax.shard_map(
        on_device, mesh=mesh, in_specs=placed, out_specs=P("dp", "sp", None), check_vma=False
    )
```

profile of v0, /device:TPU:9, one launch (start us, length us, event | category | flops | bytes accessed | tf_op | source)
XLA Modules:
  0.0 295.3 jit_solution(8072346256680333913)
XLA Ops:
  9.4 5.7 %all-to-all-start.1 = ((f32[2,128,32]{1,0,2:T(2,128)}), f32[2,128,32]{1,0,2:T(2,128)S(1)}, u32[]{:S(2)}, u32[]{:S(2)}) async-start(f32[2,128,32]{1,0,2:T(2,128)} %copy.35), calls=%async_computation.1 | async-start | bytes 65536 | tf_op jit(solution)/shard_map/all_to_all | solution.py:63
  15.1 17.9 %all-gather.7.cloned.1.call-done = bf16[2048,512]{1,0:T(8,128)(2,1)} async-done(((bf16[512,512]{1,0:T(8,128)(2,1)}), bf16[2048,512]{1,0:T(8,128)(2,1)}) %all-gather.7.cloned.1.call-update) | async-done | bytes 2097168 | tf_op jit(solution)/shard_map/all_gather | solution.py:54
  33.0 2.3 convolution_convert_fusion.4
  36.2 5.5 %all-to-all-start.2 = ((bf16[2,128,512]{1,0,2:T(2,128)(2,1)}), bf16[2,128,512]{1,0,2:T(2,128)(2,1)S(1)}, u32[]{:S(2)}, u32[]{:S(2)}) async-start(bf16[2,128,512]{1,0,2:T(2,128)(2,1)} %copy.37), calls=%async_computation.2 | async-start | bytes 524288 | tf_op jit(solution)/shard_map/all_to_all | solution.py:60
  41.7 15.5 %all-gather.9.cloned.1.call-done = bf16[2048,512]{1,0:T(8,128)(2,1)} async-done(((bf16[512,512]{1,0:T(8,128)(2,1)}), bf16[2048,512]{1,0:T(8,128)(2,1)}) %all-gather.9.cloned.1.call-update) | async-done | bytes 2097168 | tf_op jit(solution)/shard_map/all_gather | solution.py:55
  57.2 2.3 convolution_convert_fusion.3
  60.4 5.5 %all-to-all-start.3 = ((bf16[2,128,512]{1,0,2:T(2,128)(2,1)}), bf16[2,128,512]{1,0,2:T(2,128)(2,1)S(1)}, u32[]{:S(2)}, u32[]{:S(2)}) async-start(bf16[2,128,512]{1,0,2:T(2,128)(2,1)} %copy.40), calls=%async_computation.3 | async-start | bytes 524288 | tf_op jit(solution)/shard_map/all_to_all | solution.py:61
  65.9 51.2 %all-gather.5.cloned.1.call-done = bf16[2048,2048]{1,0:T(8,128)(2,1)} async-done(((bf16[512,2048]{1,0:T(8,128)(2,1)}), bf16[2048,2048]{1,0:T(8,128)(2,1)}) %all-gather.5.cloned.1.call-update) | async-done | bytes 8388624 | tf_op jit(solution)/shard_map/all_gather | solution.py:52
  117.1 5.7 %convolution_convert_fusion.2 = bf16[256,2048]{1,0:T(8,128)(2,1)S(1)} fusion(bf16[256,2048]{1,0:T(8,128)(2,1)S(1)} %bitcast.94, bf16[2048,2048]{1,0:T(8,128)(2,1)} %all-gather.5.cloned.1.call-done), kind=kOutput, calls=%fused_computation.22 | convolution fusion | flops 2148007936 | bytes 10485760 | tf_op jit(solution)/shard_map/dot_general | solution.py:44
  122.8 2.0 copy.32
  124.8 5.5 %all-to-all-start = ((bf16[2,128,2048]{1,0,2:T(2,128)(2,1)}), bf16[2,128,2048]{1,0,2:T(2,128)(2,1)S(1)}, u32[]{:S(2)}, u32[]{:S(2)}) async-start(bf16[2,128,2048]{1,0,2:T(2,128)(2,1)} %copy.32), calls=%async_computation | async-start | bytes 2097152 | tf_op jit(solution)/shard_map/all_to_all | solution.py:59
  133.7 20.2 %all-to-all-done = bf16[2,128,2048]{1,0,2:T(2,128)(2,1)S(1)} async-done(((bf16[2,128,2048]{1,0,2:T(2,128)(2,1)}), bf16[2,128,2048]{1,0,2:T(2,128)(2,1)S(1)}, u32[]{:S(2)}, u32[]{:S(2)}) %all-to-all-start) | async-done | bytes 1048608 | tf_op jit(solution)/shard_map/all_to_all | solution.py:59
  156.0 92.7 %while.33 = (s32[]{:T(128)}, bf16[2,4,1024,64]{2,3,1,0:T(8,128)(2,1)}, bf16[2,4,1024,64]{2,3,1,0:T(8,128)(2,1)}, f32[2,4,1024]{2,1,0:T(4,128)}, bf16[2,1024,64]{...) while((s32[]{:T(128)}, ...), condition=%wide.region_7.8_spmd, body=%wide.region_0.7_spmd.sunk | while | flops 142114304 | bytes 13243573 | solution.py:90
  156.0 1.9 dynamic-slice_bitcast_fusion.8
  160.7 40.4 %while.34 = (s32[]{:T(128)}, bf16[4,1024,64]{2,1,0:T(8,128)(2,1)S(1)}, bf16[4,1024,64]{2,1,0:T(8,128)(2,1)S(1)}, f32[4,1024]{1,0:T(4,128)}, bf16[1024,64]{1,0:T(...) while((s32[]{:T(128)}, ...), condition=%wide.region_6.6_spmd, body=%wide.region_1.5_spmd.sunk | while | flops 142114304 | bytes 8491452 | solution.py:88
  161.5 9.1 %while.35 = (s32[]{:T(128)}, bf16[2,512,64]{1,2,0:T(8,128)(2,1)S(1)}, s32[2]{0:T(128)S(1)}, bf16[1024,64]{1,0:T(8,128)(2,1)S(1)}, bf16[1024,64]{1,0:T(8,128)(2,1...) while((s32[]{:T(128)}, ...), condition=%wide.region_5.4_spmd.clone, body=%wide.region_2.3_spmd.clone.sunk | while | flops 142114304 | bytes 7434451 | solution.py:33
  167.4 1.7 fusion.28
  171.6 9.1 %while.35 = (s32[]{:T(128)}, bf16[2,512,64]{1,2,0:T(8,128)(2,1)S(1)}, s32[2]{0:T(128)S(1)}, bf16[1024,64]{1,0:T(8,128)(2,1)S(1)}, bf16[1024,64]{1,0:T(8,128)(2,1...) while((s32[]{:T(128)}, ...), condition=%wide.region_5.4_spmd.clone, body=%wide.region_2.3_spmd.clone.sunk | while | flops 142114304 | bytes 7434451 | solution.py:33
  181.7 9.1 %while.35 = (s32[]{:T(128)}, bf16[2,512,64]{1,2,0:T(8,128)(2,1)S(1)}, s32[2]{0:T(128)S(1)}, bf16[1024,64]{1,0:T(8,128)(2,1)S(1)}, bf16[1024,64]{1,0:T(8,128)(2,1...) while((s32[]{:T(128)}, ...), condition=%wide.region_5.4_spmd.clone, body=%wide.region_2.3_spmd.clone.sunk | while | flops 142114304 | bytes 7434451 | solution.py:33
  187.6 1.7 fusion.28
  191.8 9.1 %while.35 = (s32[]{:T(128)}, bf16[2,512,64]{1,2,0:T(8,128)(2,1)S(1)}, s32[2]{0:T(128)S(1)}, bf16[1024,64]{1,0:T(8,128)(2,1)S(1)}, bf16[1024,64]{1,0:T(8,128)(2,1...) while((s32[]{:T(128)}, ...), condition=%wide.region_5.4_spmd.clone, body=%wide.region_2.3_spmd.clone.sunk | while | flops 142114304 | bytes 7434451 | solution.py:33
  202.3 1.9 dynamic-slice_bitcast_fusion.8
  207.1 40.4 %while.34 = (s32[]{:T(128)}, bf16[4,1024,64]{2,1,0:T(8,128)(2,1)S(1)}, bf16[4,1024,64]{2,1,0:T(8,128)(2,1)S(1)}, f32[4,1024]{1,0:T(4,128)}, bf16[1024,64]{1,0:T(...) while((s32[]{:T(128)}, ...), condition=%wide.region_6.6_spmd, body=%wide.region_1.5_spmd.sunk | while | flops 142114304 | bytes 8491452 | solution.py:88
  207.8 9.1 %while.35 = (s32[]{:T(128)}, bf16[2,512,64]{1,2,0:T(8,128)(2,1)S(1)}, s32[2]{0:T(128)S(1)}, bf16[1024,64]{1,0:T(8,128)(2,1)S(1)}, bf16[1024,64]{1,0:T(8,128)(2,1...) while((s32[]{:T(128)}, ...), condition=%wide.region_5.4_spmd.clone, body=%wide.region_2.3_spmd.clone.sunk | while | flops 142114304 | bytes 7434451 | solution.py:33
  218.0 9.1 %while.35 = (s32[]{:T(128)}, bf16[2,512,64]{1,2,0:T(8,128)(2,1)S(1)}, s32[2]{0:T(128)S(1)}, bf16[1024,64]{1,0:T(8,128)(2,1)S(1)}, bf16[1024,64]{1,0:T(8,128)(2,1...) while((s32[]{:T(128)}, ...), condition=%wide.region_5.4_spmd.clone, body=%wide.region_2.3_spmd.clone.sunk | while | flops 142114304 | bytes 7434451 | solution.py:33
  228.1 9.1 %while.35 = (s32[]{:T(128)}, bf16[2,512,64]{1,2,0:T(8,128)(2,1)S(1)}, s32[2]{0:T(128)S(1)}, bf16[1024,64]{1,0:T(8,128)(2,1)S(1)}, bf16[1024,64]{1,0:T(8,128)(2,1...) while((s32[]{:T(128)}, ...), condition=%wide.region_5.4_spmd.clone, body=%wide.region_2.3_spmd.clone.sunk | while | flops 142114304 | bytes 7434451 | solution.py:33
  234.0 1.7 fusion.28
  238.2 9.1 %while.35 = (s32[]{:T(128)}, bf16[2,512,64]{1,2,0:T(8,128)(2,1)S(1)}, s32[2]{0:T(128)S(1)}, bf16[1024,64]{1,0:T(8,128)(2,1)S(1)}, bf16[1024,64]{1,0:T(8,128)(2,1...) while((s32[]{:T(128)}, ...), condition=%wide.region_5.4_spmd.clone, body=%wide.region_2.3_spmd.clone.sunk | while | flops 142114304 | bytes 7434451 | solution.py:33
  244.1 1.7 fusion.28
  248.7 2.5 copy.47
  251.2 29.9 %all_to_all.81 = bf16[2,1024,256]{2,0,1:T(2,128)(2,1)S(1)} all-to-all(bf16[2,1024,256]{2,0,1:T(2,128)(2,1)S(1)} %copy.47), channel_id=1, replica_groups=mesh['sp'=8,'dp'=4] {'sp'}, dimensions={1} | all-to-all | bytes 2097152 | tf_op jit(solution)/shard_map/all_to_all | solution.py:95
  282.0 6.7 %convolution_convert_fusion.1 = bf16[256,2048]{1,0:T(8,128)(2,1)} fusion(bf16[256,2048]{1,0:T(8,128)(2,1)S(1)} %bitcast.107, bf16[2048,2048]{1,0:T(8,128)(2,1)} %all-gather.11.cloned.1.call-done), kind=kOutput, calls=%fused_computation.21 | convolution fusion | flops 2148007936 | bytes 10485760 | tf_op jit(solution)/shard_map/dot_general | solution.py:97
  (215 shorter events, 81.9 us)
Async XLA Ops:
  6.5 26.5 %copy-start = (bf16[2,128,2048]{2,1,0:T(8,128)(2,1)S(1)}, bf16[2,128,2048]{2,1,0:T(8,128)(2,1)}, u32[]{:S(2)}) copy-start(bf16[2,128,2048]{2,1,0:T(8,128)(2,1)} %param.12) | copy-start | bytes 3145732
  6.5 2.2 copy-start.2
  6.5 26.5 %all-gather.7.cloned.1.call-start = ((), (), s32[]{:S(2)}) async-start(), calls=%async_computation.6 | async-start | bytes 2621440 | tf_op jit(solution)/shard_map/all_gather | solution.py:54
  7.3 49.9 %all-gather.9.cloned.1.call-start = ((), (), s32[]{:S(2)}) async-start(), calls=%async_computation.7 | async-start | bytes 2621440 | tf_op jit(solution)/shard_map/all_gather | solution.py:55
  8.0 109.1 %all-gather.5.cloned.1.call-start = ((), (), s32[]{:S(2)}) async-start(), calls=%async_computation.5 | async-start | bytes 10485760 | tf_op jit(solution)/shard_map/all_gather | solution.py:52
  9.4 26.8 %all-to-all-start.1 = ((f32[2,128,32]{1,0,2:T(2,128)}), f32[2,128,32]{1,0,2:T(2,128)S(1)}, u32[]{:S(2)}, u32[]{:S(2)}) async-start(f32[2,128,32]{1,0,2:T(2,128)} %copy.35), calls=%async_computation.1 | async-start | bytes 65536 | tf_op jit(solution)/shard_map/all_to_all | solution.py:63
  36.2 24.1 %all-to-all-start.2 = ((bf16[2,128,512]{1,0,2:T(2,128)(2,1)}), bf16[2,128,512]{1,0,2:T(2,128)(2,1)S(1)}, u32[]{:S(2)}, u32[]{:S(2)}) async-start(bf16[2,128,512]{1,0,2:T(2,128)(2,1)} %copy.37), calls=%async_computation.2 | async-start | bytes 524288 | tf_op jit(solution)/shard_map/all_to_all | solution.py:60
  60.4 64.4 %all-to-all-start.3 = ((bf16[2,128,512]{1,0,2:T(2,128)(2,1)}), bf16[2,128,512]{1,0,2:T(2,128)(2,1)S(1)}, u32[]{:S(2)}, u32[]{:S(2)}) async-start(bf16[2,128,512]{1,0,2:T(2,128)(2,1)} %copy.40), calls=%async_computation.3 | async-start | bytes 524288 | tf_op jit(solution)/shard_map/all_to_all | solution.py:61
  124.8 29.1 %all-to-all-start = ((bf16[2,128,2048]{1,0,2:T(2,128)(2,1)}), bf16[2,128,2048]{1,0,2:T(2,128)(2,1)S(1)}, u32[]{:S(2)}, u32[]{:S(2)}) async-start(bf16[2,128,2048]{1,0,2:T(2,128)(2,1)} %copy.32), calls=%async_computation | async-start | bytes 2097152 | tf_op jit(solution)/shard_map/all_to_all | solution.py:59
  130.3 151.7 %all-gather.11.cloned.1.call-start = ((), (), s32[]{:S(2)}) async-start(), calls=%async_computation.8 | async-start | bytes 10485760 | tf_op jit(solution)/shard_map/all_gather | solution.py:99
  162.8 2.4 copy-start.1
  167.4 2.4 copy-start.1
  173.0 2.4 copy-start.1
  177.5 2.4 copy-start.1
  183.1 2.4 copy-start.1
  187.6 2.4 copy-start.1
  193.2 2.4 copy-start.1
  197.7 2.4 copy-start.1
  209.2 2.4 copy-start.1
  213.7 2.4 copy-start.1
  219.3 2.4 copy-start.1
  223.9 2.4 copy-start.1
  229.4 2.4 copy-start.1
  234.0 2.4 copy-start.1
  239.5 2.4 copy-start.1
  244.1 2.4 copy-start.1
Sparse Core Ops, SparseCore 0:
  8.9 24.0 all-gather.6
  34.6 22.5 all-gather.8
  58.8 58.2 all-gather.4
  132.3 58.7 all-gather.10
where the time goes:
time: 300 us; the launch traced here: 295 us
  waiting for transfers between devices  107 us (36%)
  matrix products  57.2 us (19%)
  local copies, waits for them, and re-layouts  43.4 us (14%)
  blocking collectives  29.9 us (10%)
  starting transfers between devices  22.3 us (7%)
  between operations  13.2 us (4%)
  loops' own time  11.1 us (4%)
  other arithmetic  10.6 us (4%)
    all_gather x1, waiting for transfers between devices, on_device(): summed = absorb(lax.all_gather(query_weight, 'dp', axis=0, tiled=True))  51.2 us
    all_to_all x1, blocking collectives, on_device(): lax.all_to_all(attended, 'sp', split_axis=1, concat_axis=2, tiled=True)  29.9 us
    dot_general x16, matrix products, one_block(): jnp.dot(query_block, key_head.T, preferred_element_type=jnp.float32)  27.7 us
    all_to_all x1, waiting for transfers between devices, on_device(): lax.all_to_all(query_local, 'sp', split_axis=2, concat_axis=1, tiled=True)  20.2 us
    all_gather x1, waiting for transfers between devices, on_device(): key_sum = absorb(lax.all_gather(key_weight, 'dp', axis=0, tiled=True))  17.9 us
    all_gather x1, waiting for transfers between devices, on_device(): value_sum = absorb(lax.all_gather(value_weight, 'dp', axis=0, tiled=True))  15.5 us
    dot_general x16, matrix products, one_block(): jnp.dot(weights, value_head, preferred_element_type=jnp.float32)  12.6 us
    another operation x8, loops' own time, attend_one(): result = lax.map(one_block, jnp.arange(block_count, dtype=jnp.int32))  10.7 us
  transfers between devices with their start and end apart: 8, of which 4 were waited for; matrix products, arithmetic and copies ran while one was open for 35% of the time, Pallas kernels for 0%

commit v1 on v0

v1 whole, which is shorter than its diff:
```python
import functools
import math

import jax
import jax.numpy as jnp
from jax import lax
from jax.experimental import pallas as pl
from jax.experimental.pallas import tpu as pltpu
from jax.sharding import PartitionSpec as P

KV_HEADS = 8
HEAD = 64


def attend_rows(q, k_of, v_of, gate_column, gate_row_of, start, rows):
    scaled = q * jnp.asarray(HEAD**-0.5, q.dtype)
    contract = (((1,), (1,)), ((), ()))

    def scores(lo, hi):
        product = lax.dot_general(scaled, k_of(lo, hi), contract, preferred_element_type=jnp.float32)
        return product + (gate_column - gate_row_of(lo, hi))

    diagonal = scores(start, start + rows)
    row = lax.broadcasted_iota(jnp.int32, diagonal.shape, 0)
    column = lax.broadcasted_iota(jnp.int32, diagonal.shape, 1)
    diagonal = jnp.where(column <= row, diagonal, -jnp.inf)
    top = jnp.max(diagonal, axis=1, keepdims=True)
    if start:
        before = scores(0, start)
        top = jnp.maximum(top, jnp.max(before, axis=1, keepdims=True))
    raised = jnp.exp(diagonal - top)
    total = jnp.sum(raised, axis=1, keepdims=True)
    mixed = jnp.dot(raised.astype(jnp.bfloat16), v_of(start, start + rows), preferred_element_type=jnp.float32)
    if start:
        raised = jnp.exp(before - top)
        total = total + jnp.sum(raised, axis=1, keepdims=True)
        mixed = mixed + jnp.dot(raised.astype(jnp.bfloat16), v_of(0, start), preferred_element_type=jnp.float32)
    return (mixed / total).astype(jnp.bfloat16)


def attention_kernel(per_pair, q_ref, k_ref, v_ref, gate_ref, row_ref, out_ref):
    length = q_ref.shape[1]
    heads = q_ref.shape[2] // HEAD
    rows = math.gcd(length, 256)
    if length <= 1024:
        for block in range(length // rows):
            start = block * rows
            for head in range(heads):
                pair = head // per_pair
                out_ref[0, start : start + rows, head * HEAD : (head + 1) * HEAD] = attend_rows(
                    q_ref[0, start : start + rows, head * HEAD : (head + 1) * HEAD],
                    lambda lo, hi: k_ref[0, lo:hi, pair * HEAD : (pair + 1) * HEAD],
                    lambda lo, hi: v_ref[0, lo:hi, pair * HEAD : (pair + 1) * HEAD],
                    gate_ref[0, start : start + rows, head : head + 1],
                    lambda lo, hi: row_ref[0, head : head + 1, lo:hi],
                    start,
                    rows,
                )
        return
    contract = (((1,), (1,)), ((), ()))
    for head in range(heads):
        pair = head // per_pair

        def one_block(block, nothing):
            start = pl.multiple_of(block * rows, rows)
            q = q_ref[0, pl.ds(start, rows), head * HEAD : (head + 1) * HEAD]
            scaled = q * jnp.asarray(HEAD**-0.5, q.dtype)
            column = gate_ref[0, pl.ds(start, rows), head : head + 1]

            def step(other, carry):
                top, total, mixed = carry
                lo = pl.multiple_of(other * rows, rows)
                k = k_ref[0, pl.ds(lo, rows), pair * HEAD : (pair + 1) * HEAD]
                v = v_ref[0, pl.ds(lo, rows), pair * HEAD : (pair + 1) * HEAD]
                s = lax.dot_general(scaled, k, contract, preferred_element_type=jnp.float32)
                s = s + (column - row_ref[0, head : head + 1, pl.ds(lo, rows)])
                at = lax.broadcasted_iota(jnp.int32, s.shape, 0) + start
                to = lax.broadcasted_iota(jnp.int32, s.shape, 1) + lo
                s = jnp.where(to <= at, s, -jnp.inf)
                new = jnp.maximum(top, jnp.max(s, axis=1, keepdims=True))
                raised = jnp.exp(s - new)
                keep = jnp.exp(top - new)
                total = total * keep + jnp.sum(raised, axis=1, keepdims=True)
                part = jnp.dot(raised.astype(jnp.bfloat16), v, preferred_element_type=jnp.float32)
                return new, total, mixed * keep + part

            first = (
                jnp.full((rows, 1), -jnp.inf, jnp.float32),
                jnp.zeros((rows, 1), jnp.float32),
                jnp.zeros((rows, HEAD), jnp.float32),
            )
            _, total, mixed = lax.fori_loop(0, block + 1, step, first)
            out_ref[0, pl.ds(start, rows), head * HEAD : (head + 1) * HEAD] = (mixed / total).astype(jnp.bfloat16)
            return nothing

        lax.fori_loop(0, length // rows, one_block, 0)


def attention(query, key, value, gates):
    sequences, length, width = query.shape
    heads = width // HEAD
    pairs = key.shape[2] // HEAD
    whole = lambda n, c: pl.BlockSpec((1, n, c), lambda i: (i, 0, 0))
    return pl.pallas_call(
        functools.partial(attention_kernel, heads // pairs),
        grid=(sequences,),
        out_shape=jax.ShapeDtypeStruct(query.shape, jnp.bfloat16),
        in_specs=[
            whole(length, width),
            whole(length, pairs * HEAD),
            whole(length, pairs * HEAD),
            whole(length, heads),
            whole(heads, length),
        ],
        out_specs=whole(length, width),
        compiler_params=pltpu.CompilerParams(vmem_limit_bytes=40 * 1024 * 1024),
    )(query, key, value, gates, jnp.swapaxes(gates, 1, 2))


def on_device(hidden_states, cumulative_gate, query_weight, key_weight, value_weight, out_weight):
    sequences, positions, model_width = hidden_states.shape
    rows = sequences * positions
    token_rows = hidden_states.reshape(rows, model_width)
    width_query = query_weight.shape[1]
    devices = lax.axis_size("sp")
    copies = max(1, devices // KV_HEADS)

    joined = jnp.concatenate([query_weight, key_weight, value_weight], axis=1)
    joined = lax.all_gather(joined, "dp", axis=0, tiled=True)
    summed = jnp.dot(token_rows, joined, preferred_element_type=jnp.float32).astype(jnp.bfloat16)
    width_key = key_weight.shape[1]

    def spread(matrix):
        matrix = matrix.reshape(sequences, positions, KV_HEADS, HEAD)
        return jnp.repeat(matrix, copies, axis=2).reshape(sequences, positions, devices, -1)

    parts = (
        summed[:, :width_query].reshape(sequences, positions, devices, -1),
        spread(summed[:, width_query : width_query + width_key]),
        spread(summed[:, width_query + width_key :]),
    )
    sent = jnp.concatenate(parts, axis=3)
    got = lax.all_to_all(sent, "sp", split_axis=2, concat_axis=1, tiled=True)
    got = got.reshape(sequences, positions * devices, -1)
    gates = lax.all_to_all(cumulative_gate, "sp", split_axis=2, concat_axis=1, tiled=True)
    own = parts[0].shape[3]
    pair = parts[1].shape[3]
    attended = attention(got[..., :own], got[..., own : own + pair], got[..., own + pair :], gates)
    returned = lax.all_to_all(attended, "sp", split_axis=1, concat_axis=2, tiled=True)
    mixed = jnp.dot(
        returned.reshape(rows, width_query),
        lax.all_gather(out_weight, "dp", axis=0, tiled=True),
        preferred_element_type=jnp.float32,
    )
    return mixed.astype(jnp.bfloat16).reshape(sequences, positions, model_width)


def solution(mesh):
    placed = (
        P("dp", "sp", None),
        P("dp", "sp", None),
        P("dp", None),
        P("dp", None),
        P("dp", None),
        P("dp", None),
    )
    return jax.shard_map(
        on_device, mesh=mesh, in_specs=placed, out_specs=P("dp", "sp", None), check_vma=False
    )
```

time: 300 us -> 216 us (0.72)
  matrix products: 57.2 us -> 15 us
  local copies, waits for them, and re-layouts: 43.4 us -> 8.16 us
  Pallas kernels: 0 us -> 16 us
  loops' own time: 11.1 us -> 0 us
  starting transfers between devices: 22.3 us -> 11.3 us
  waiting for transfers between devices: 107 us -> 112 us
  other arithmetic: 10.6 us -> 6.15 us
    dot_general x36 -> x2, matrix products: 57.2 us -> 15 us  [the longest x1 8.3 us: on_device(): jnp.dot(token_rows, joined, preferred_element_type=jnp.float32)]
    dynamic_slice x44 -> x0, local copies, waits for them, and re-layouts: 20.1 us -> none  [the longest x16 9.92 us: attend_one(): result = lax.map(one_block, jnp.arange(block_count, dtype=jnp.int32))]
    pallas_call x0 -> x1, Pallas kernels: none -> 16 us  [attention(): pl.pallas_call(functools.partial(attention_kernel, heads // pairs), grid=...]
    all_to_all x3 -> x1, waiting for transfers between devices: 20.2 us -> 34.9 us  [on_device(): got = lax.all_to_all(sent, 'sp', split_axis=2, concat_axis=1, tiled=True)]
    another operation x11 -> x0, loops' own time: 11.1 us -> none  [the longest x8 10.7 us: attend_one(): result = lax.map(one_block, jnp.arange(block_count, dtype=jnp.int32))]
    all_to_all x3 -> x1, starting transfers between devices: 16.5 us -> 5.49 us  [on_device(): got = lax.all_to_all(sent, 'sp', split_axis=2, concat_axis=1, tiled=True)]
    reduce_sum x16 -> x0, other arithmetic: 10.6 us -> none  [one_block(): jnp.sum(exponent, axis=1, keepdims=True)]
    all_gather x3 -> x1, waiting for transfers between devices: 84.6 us -> 76.7 us  [on_device(): joined = lax.all_gather(joined, 'dp', axis=0, tiled=True)]
  transfers between devices with their start and end apart: 8 -> 4, of which waited for: 4 -> 2; matrix products, arithmetic and copies ran while one was open for 35% -> 9% of each run, Pallas kernels for 0% -> 8%
where the time goes in v1:
time: 216 us; the launch traced here: 212 us
  waiting for transfers between devices  112 us (52%)
  blocking collectives  29.4 us (14%)
  Pallas kernels  16 us (7%)
  matrix products  15 us (7%)
  between operations  13.5 us (6%)
  starting transfers between devices  11.3 us (5%)
  local copies, waits for them, and re-layouts  8.16 us (4%)
  other arithmetic  6.15 us (3%)
    all_gather x1, waiting for transfers between devices, on_device(): joined = lax.all_gather(joined, 'dp', axis=0, tiled=True)  76.7 us
    all_to_all x1, waiting for transfers between devices, on_device(): got = lax.all_to_all(sent, 'sp', split_axis=2, concat_axis=1, tiled=True)  34.9 us
    all_to_all x1, blocking collectives, on_device(): lax.all_to_all(attended, 'sp', split_axis=1, concat_axis=2, tiled=True)  29.4 us
    pallas_call x1, Pallas kernels, attention(): pl.pallas_call(functools.partial(attention_kernel, heads // pairs), grid=...  16 us
    dot_general x1, matrix products, on_device(): jnp.dot(token_rows, joined, preferred_element_type=jnp.float32)  8.3 us
    dot_general x1, matrix products, on_device(): jnp.dot(returned.reshape(rows, width_query), lax.all_gather(out_weight, '...  6.68 us
    all_to_all x1, starting transfers between devices, on_device(): lax.all_to_all(cumulative_gate, 'sp', split_axis=2, concat_axis=1, tiled=...  5.72 us
    all_to_all x1, starting transfers between devices, on_device(): got = lax.all_to_all(sent, 'sp', split_axis=2, concat_axis=1, tiled=True)  5.49 us
  transfers between devices with their start and end apart: 4, of which 2 were waited for; matrix products, arithmetic and copies ran while one was open for 9% of the time, Pallas kernels for 8%

profile of v1, /device:TPU:9, one launch (start us, length us, event | category | flops | bytes accessed | tf_op | source)
XLA Modules:
  0.0 211.8 jit_solution(14432660612491214772)
XLA Ops:
  6.5 0.0 copy-start
  6.5 0.0 all-gather.3.cloned.1.call-start
  6.5 3.3 %pad_maximum_fusion = bf16[512,3072]{1,0:T(8,128)(2,1)} fusion(bf16[512,512]{1,0:T(8,128)(2,1)} %param.10, bf16[512,512]{1,0:T(8,128)(2,1)} %param.9, bf16[512,2048]{1,0:T(8,128)(2,1)} %param.8), kind=kLoop, calls=%fused_computation.2 | loop fusion | flops 9437184 | bytes 6291456 | tf_op jit(solution)/shard_map/concatenate | solution.py:128
  9.8 0.0 all-gather.3.cloned.1.call-update
  9.9 0.0 all-gather.5.cloned.1.call-start
  9.9 0.7 all-gather.5.cloned.1.call-update
  10.6 0.6 copy.22
  11.3 5.7 %all-to-all-start.1 = ((f32[2,128,32]{1,0,2:T(2,128)}), f32[2,128,32]{1,0,2:T(2,128)S(1)}, u32[]{:S(2)}, u32[]{:S(2)}) async-start(f32[2,128,32]{1,0,2:T(2,128)} %copy.22), calls=%async_computation.1 | async-start | bytes 65536 | tf_op jit(solution)/shard_map/all_to_all | solution.py:145
  17.0 76.7 %all-gather.3.cloned.1.call-done = bf16[2048,3072]{1,0:T(8,128)(2,1)} async-done(((bf16[512,3072]{1,0:T(8,128)(2,1)}), bf16[2048,3072]{1,0:T(8,128)(2,1)}) %all-gather.3.cloned.1.call-update) | async-done | bytes 12582928 | tf_op jit(solution)/shard_map/all_gather | solution.py:129
  93.7 8.3 %fusion = bf16[256,3072]{0,1:T(8,128)(2,1)S(1)} fusion(bf16[2048,3072]{1,0:T(8,128)(2,1)} %all-gather.3.cloned.1.call-done, bf16[256,2048]{1,0:T(8,128)(2,1)S(1)} %bitcast.32), kind=kOutput, calls=%fused_computation.1 | convolution fusion | flops 3222011904 | bytes 15204352 | tf_op jit(solution)/shard_map/dot_general | solution.py:130
  102.0 0.1 slice.24
  102.1 0.1 reshape_broadcast_in_dim_reshape.6
  102.2 1.0 copy.19
  103.2 0.1 reshape_broadcast_in_dim_reshape.7
  103.3 1.0 copy.20
  104.3 0.3 reshape.18
  104.6 0.7 copy.18
  105.3 2.9 %pad_maximum_fusion.1 = bf16[2,128,8,384]{3,1,0,2:T(8,128)(2,1)} fusion(bf16[2,128,8,64]{3,1,0,2:T(8,128)(2,1)} %copy.20, bf16[2,128,8,64]{3,1,0,2:T(8,128)(2,1)} %copy.19, bf16[2,128,8,256]{3,1,0,2:T(8,128)(2,1)S(1)} %copy.18), kind=kLoop, calls=%fused_computation.4 | loop fusion | flops 4718592 | bytes 3145728 | tf_op jit(solution)/shard_map/concatenate | solution.py:142
  108.1 0.0 all-to-all-done.1
  108.1 5.5 %all-to-all-start = ((bf16[2,128,8,384]{3,1,0,2:T(8,128)(2,1)}), bf16[2,128,8,384]{3,1,0,2:T(8,128)(2,1)}, u32[]{:S(2)}, u32[]{:S(2)}) async-start(bf16[2,128,8,384]{3,1,0,2:T(8,128)(2,1)} %pad_maximum_fusion.1), calls=%async_computation | async-start | bytes 3145728 | tf_op jit(solution)/shard_map/all_to_all | solution.py:143
  113.7 0.4 copy.24.gate_ref
  114.0 34.9 %all-to-all-done = bf16[2,128,8,384]{3,1,0,2:T(8,128)(2,1)} async-done(((bf16[2,128,8,384]{3,1,0,2:T(8,128)(2,1)}), bf16[2,128,8,384]{3,1,0,2:T(8,128)(2,1)}, u32[]{:S(2)}, u32[]{:S(2)}) %all-to-all-start) | async-done | bytes 1572896 | tf_op jit(solution)/shard_map/all_to_all | solution.py:143
  148.9 1.6 copy.21
  150.5 0.1 slice.27.q_ref
  150.6 0.2 fusion.1
  150.9 16.0 %shard_map.64 = bf16[2,1024,256]{2,1,0:T(8,128)(2,1)S(1)} custom-call(bf16[2,1024,256]{2,1,0:T(8,128)(2,1)S(1)} %slice.27.q_ref, bf16[2,1024,64]{2,1,0:T(8,128)(2,1)S(1)} %get-tuple-element.6.k_ref, bf16[2,1024,64]{2,1,0:T(8,128)(2,1)S(1)} %get-tuple-element.5.v_ref, f32[2,1024,4]{2,1,0:T(8,128)S(1)} %copy.24.gate_ref, f32[2,4,1024]{2,1,0:T(4,128)S(1)} %bitcast.33), custom_call_target="tpu_custom_call" | custom-call | tf_op jit(solution)/shard_map/pallas_call | solution.py:104
  166.9 1.1 copy.25
  168.0 29.4 %all_to_all.48 = bf16[2,1024,256]{2,0,1:T(2,128)(2,1)S(1)} all-to-all(bf16[2,1024,256]{2,0,1:T(2,128)(2,1)S(1)} %copy.25), channel_id=1, replica_groups=mesh['sp'=8,'dp'=4] {'sp'}, dimensions={1} | all-to-all | bytes 2097152 | tf_op jit(solution)/shard_map/all_to_all | solution.py:149
  197.4 0.6 copy.26
  198.0 0.3 copy.27
  198.3 0.0 all-gather.5.cloned.1.call-done
  198.3 6.7 %convolution_convert_fusion.1 = bf16[256,2048]{1,0:T(8,128)(2,1)} fusion(bf16[256,2048]{1,0:T(8,128)(2,1)S(1)} %bitcast.38, bf16[2048,2048]{1,0:T(8,128)(2,1)} %all-gather.5.cloned.1.call-done), kind=kOutput, calls=%fused_computation.3 | convolution fusion | flops 2148007936 | bytes 10485760 | tf_op jit(solution)/shard_map/dot_general | solution.py:150
  (6 shorter events, 0.1 us)
Async XLA Ops:
  6.5 87.1 %copy-start = (bf16[2,128,2048]{2,1,0:T(8,128)(2,1)S(1)}, bf16[2,128,2048]{2,1,0:T(8,128)(2,1)}, u32[]{:S(2)}) copy-start(bf16[2,128,2048]{2,1,0:T(8,128)(2,1)} %param.6) | copy-start | bytes 3145732
  6.5 87.1 %all-gather.3.cloned.1.call-start = ((), (), s32[]{:S(2)}) async-start(), calls=%async_computation.3 | async-start | bytes 15728640 | tf_op jit(solution)/shard_map/all_gather | solution.py:129
  9.8 0.8 copy-start.1
  9.9 188.5 %all-gather.5.cloned.1.call-start = ((), (), s32[]{:S(2)}) async-start(), calls=%async_computation.4 | async-start | bytes 10485760 | tf_op jit(solution)/shard_map/all_gather | solution.py:152
  11.3 96.9 %all-to-all-start.1 = ((f32[2,128,32]{1,0,2:T(2,128)}), f32[2,128,32]{1,0,2:T(2,128)S(1)}, u32[]{:S(2)}, u32[]{:S(2)}) async-start(f32[2,128,32]{1,0,2:T(2,128)} %copy.22), calls=%async_computation.1 | async-start | bytes 65536 | tf_op jit(solution)/shard_map/all_to_all | solution.py:145
  108.1 40.8 %all-to-all-start = ((bf16[2,128,8,384]{3,1,0,2:T(8,128)(2,1)}), bf16[2,128,8,384]{3,1,0,2:T(8,128)(2,1)}, u32[]{:S(2)}, u32[]{:S(2)}) async-start(bf16[2,128,8,384]{3,1,0,2:T(8,128)(2,1)} %pad_maximum_fusion.1), calls=%async_computation | async-start | bytes 3145728 | tf_op jit(solution)/shard_map/all_to_all | solution.py:143
Sparse Core Ops, SparseCore 0:
  10.0 83.6 all-gather.2
  95.2 58.2 all-gather.4

commit v2 on v1

v2 whole, which is shorter than its diff:
```python
import functools
import math

import jax
import jax.numpy as jnp
from jax import lax
from jax.experimental import pallas as pl
from jax.experimental.pallas import tpu as pltpu
from jax.sharding import PartitionSpec as P

KV_HEADS = 8
HEAD = 64


def attend_rows(q, k_of, v_of, gate_column, gate_row_of, start, rows):
    scaled = q * jnp.asarray(HEAD**-0.5, q.dtype)
    contract = (((1,), (1,)), ((), ()))

    def scores(lo, hi):
        product = lax.dot_general(scaled, k_of(lo, hi), contract, preferred_element_type=jnp.float32)
        return product + (gate_column - gate_row_of(lo, hi))

    diagonal = scores(start, start + rows)
    row = lax.broadcasted_iota(jnp.int32, diagonal.shape, 0)
    column = lax.broadcasted_iota(jnp.int32, diagonal.shape, 1)
    diagonal = jnp.where(column <= row, diagonal, -jnp.inf)
    top = jnp.max(diagonal, axis=1, keepdims=True)
    if start:
        before = scores(0, start)
        top = jnp.maximum(top, jnp.max(before, axis=1, keepdims=True))
    raised = jnp.exp(diagonal - top)
    total = jnp.sum(raised, axis=1, keepdims=True)
    mixed = jnp.dot(raised.astype(jnp.bfloat16), v_of(start, start + rows), preferred_element_type=jnp.float32)
    if start:
        raised = jnp.exp(before - top)
        total = total + jnp.sum(raised, axis=1, keepdims=True)
        mixed = mixed + jnp.dot(raised.astype(jnp.bfloat16), v_of(0, start), preferred_element_type=jnp.float32)
    return (mixed / total).astype(jnp.bfloat16)


def attend_long(q_of, k_of, v_of, gate_column_of, gate_row_of, store, length, rows):
    contract = (((1,), (1,)), ((), ()))

    def one_block(block, nothing):
        start = pl.multiple_of(block * rows, rows)
        q = q_of(start, rows)
        scaled = q * jnp.asarray(HEAD**-0.5, q.dtype)
        column = gate_column_of(start, rows)

        def step(other, carry):
            top, total, mixed = carry
            lo = pl.multiple_of(other * rows, rows)
            s = lax.dot_general(scaled, k_of(lo, rows), contract, preferred_element_type=jnp.float32)
            s = s + (column - gate_row_of(lo, rows))
            at = lax.broadcasted_iota(jnp.int32, s.shape, 0) + start
            to = lax.broadcasted_iota(jnp.int32, s.shape, 1) + lo
            s = jnp.where(to <= at, s, -jnp.inf)
            new = jnp.maximum(top, jnp.max(s, axis=1, keepdims=True))
            raised = jnp.exp(s - new)
            keep = jnp.exp(top - new)
            total = total * keep + jnp.sum(raised, axis=1, keepdims=True)
            part = jnp.dot(raised.astype(jnp.bfloat16), v_of(lo, rows), preferred_element_type=jnp.float32)
            return new, total, mixed * keep + part

        first = (
            jnp.full((rows, 1), -jnp.inf, jnp.float32),
            jnp.zeros((rows, 1), jnp.float32),
            jnp.zeros((rows, HEAD), jnp.float32),
        )
        _, total, mixed = lax.fori_loop(0, block + 1, step, first)
        store(block, (mixed / total).astype(jnp.bfloat16))
        return nothing

    lax.fori_loop(0, length // rows, one_block, 0)


class Gather:
    def __init__(self, buf, n, m, me, sems):
        self.buf, self.n, self.m = buf, n, m
        self.s, self.d = me
        self.have, self.partner_have, self.own_recv, self.send_a, self.send_b, self.send_c, self.own_send = sems
        self.partner = self.d + 1 - 2 * lax.rem(self.d, 2)
        self.y, self.z = lax.rem(self.s, 2), self.s // 2
        self.big = n // 2
        self.r1, self.r2 = split_rows(buf.shape[1], n)
        self.started = []
        self.mirrors = range(1, m // 2)

    def rows_pair(self, y):
        return pl.ds(pl.multiple_of(y * self.r1, 16), self.r1)

    def rows_many(self, z):
        return pl.ds(pl.multiple_of(2 * self.r1 + z * self.r2, 16), self.r2)

    def go(self, part, send, recv, device):
        copy = pltpu.make_async_remote_copy(
            src_ref=part, dst_ref=part, send_sem=send, recv_sem=recv, device_id=device,
            device_id_type=pl.DeviceIdType.MESH,
        )
        copy.start()
        self.started.append(copy)

    def take(self, part, recv):
        pltpu.make_async_remote_copy(
            src_ref=part, dst_ref=part, send_sem=self.own_send, recv_sem=recv, device_id=(self.s, self.partner),
            device_id_type=pl.DeviceIdType.MESH,
        ).wait_recv()

    def cross(self):
        for t in self.mirrors:
            to = (self.s, lax.rem(self.d + 2 * t, self.m))
            self.go(self.buf.at[self.d, self.rows_pair(self.y)], self.send_a.at[t, 0], self.have.at[t, self.y], to)
            if self.r2:
                self.go(
                    self.buf.at[self.d, self.rows_many(self.z)], self.send_a.at[t, 1], self.have.at[t, 2 + self.z], to
                )

    def to_partner(self):
        self.go(self.buf.at[self.d], self.own_send, self.own_recv, (self.s, self.partner))

    def take_partner(self):
        self.take(self.buf.at[self.partner], self.own_recv)

    def source(self, t):
        return lax.rem(self.d - 2 * t + self.m, self.m)

    def share(self):
        for t in self.mirrors:
            e = self.source(t)
            part = self.buf.at[e, self.rows_pair(self.y)]
            self.take(part, self.have.at[t, self.y])
            self.go(part, self.send_b.at[t, 0], self.have.at[t, self.y], (self.s + 1 - 2 * self.y, self.d))
            if self.r2:
                part = self.buf.at[e, self.rows_many(self.z)]
                self.take(part, self.have.at[t, 2 + self.z])
                for k in range(1, self.big):
                    to = (lax.rem(self.z + k, self.big) * 2 + self.y, self.d)
                    self.go(part, self.send_b.at[t, k], self.have.at[t, 2 + self.z], to)
            part = self.buf.at[e, self.rows_pair(self.y)]
            self.pass_on(part, t, self.y)
            if self.r2:
                self.pass_on(self.buf.at[e, self.rows_many(self.z)], t, 2 + self.z)

    def pass_on(self, part, t, c):
        self.go(part, self.send_c.at[t, c], self.partner_have.at[t, c], (self.s, self.partner))

    def collect(self):
        for t in self.mirrors:
            e = self.source(t)
            c = 1 - self.y
            part = self.buf.at[e, self.rows_pair(c)]
            self.take(part, self.have.at[t, c])
            self.pass_on(part, t, c)
            if self.r2:
                for k in range(1, self.big):
                    c = lax.rem(self.z + k, self.big)
                    part = self.buf.at[e, self.rows_many(c)]
                    self.take(part, self.have.at[t, 2 + c])
                    self.pass_on(part, t, 2 + c)

    def finish(self, t):
        e = self.source(t)
        other = e + 1 - 2 * lax.rem(e, 2)
        for c in range(2):
            self.take(self.buf.at[other, self.rows_pair(c)], self.partner_have.at[t, c])
        if self.r2:
            for c in range(self.big):
                self.take(self.buf.at[other, self.rows_many(c)], self.partner_have.at[t, 2 + c])
        return other

    def drain(self):
        for copy in self.started:
            copy.wait_send()


def split_rows(rows, n):
    big = n // 2
    many = rows * 5 // 8 // big // 16 * 16
    return (rows - many * big) // 2, many


def gather_sems(n, m):
    dma = pltpu.SemaphoreType.DMA
    t, c = max(m // 2, 2), 2 + n // 2
    return [dma((t, c)), dma((t, c)), dma, dma((t, 2)), dma((t, max(2, n // 2))), dma((t, c)), dma]


def layer_kernel(n, m, sequences, heads, pairs, hidden, gates, wq, wk, wv, wo, out,
                 qkv, outw, summed, send, got, gate_got, gate_row, gate_column, keys, values, att, ret, lhs, *sems):
    s, d = lax.axis_index("sp"), lax.axis_index("dp")
    first, second = sems[:7], sems[7:14]
    local, gate_send, gate_recv, q_send, q_recv, r_send, r_recv = sems[14:]
    positions = hidden.shape[0] // sequences
    length = positions * n
    mesh_id = pl.DeviceIdType.MESH
    one = Gather(qkv, n, m, (s, d), first)
    two = Gather(outw, n, m, (s, d), second)
    width_q, width_k = wq.shape[1], wk.shape[1]

    inward = [
        pltpu.make_async_copy(wq, qkv.at[d, :, pl.ds(0, width_q)], local.at[0]),
        pltpu.make_async_copy(wk, qkv.at[d, :, pl.ds(width_q, width_k)], local.at[1]),
        pltpu.make_async_copy(wv, qkv.at[d, :, pl.ds(width_q + width_k, width_k)], local.at[2]),
        pltpu.make_async_copy(wo, outw.at[d], local.at[3]),
        pltpu.make_async_copy(gates.at[s], gate_got.at[s], local.at[4]),
    ]
    for copy in inward:
        copy.start()
    barrier = pltpu.get_barrier_semaphore()
    for k in range(1, n):
        pl.semaphore_signal(barrier, inc=1, device_id=(lax.rem(s + k, n), d), device_id_type=mesh_id)
    for k in range(1, m):
        pl.semaphore_signal(barrier, inc=1, device_id=(s, lax.rem(d + k, m)), device_id_type=mesh_id)
    pl.semaphore_wait(barrier, n - 1 + m - 1)

    def exchange(source, target, send_sem, recv_sem):
        copies = []
        for k in range(1, n):
            to = lax.rem(s + k, n)
            copy = pltpu.make_async_remote_copy(
                src_ref=source(to), dst_ref=target(s), send_sem=send_sem(k), recv_sem=recv_sem(n - k),
                device_id=(to, d), device_id_type=mesh_id,
            )
            copy.start()
            copies.append(copy)
        return copies

    def arrive(target, send_sem, recv_sem):
        for k in range(1, n):
            block = target(lax.rem(s + k, n))
            pltpu.make_async_remote_copy(
                src_ref=block, dst_ref=block, send_sem=send_sem(k), recv_sem=recv_sem(k),
                device_id=(lax.rem(s + k, n), d), device_id_type=mesh_id,
            ).wait_recv()

    for copy in inward[:3]:
        copy.wait()
    one.cross()
    one.to_partner()
    gate_args = lambda j: gates.at[j], lambda j: gate_got.at[j], lambda k: gate_send.at[k], lambda k: gate_recv.at[k]
    gate_copies = exchange(*gate_args)

    depth = qkv.shape[1]
    tile = math.gcd(qkv.shape[2], 512)

    def project(e, begin):
        columns = hidden[:, pl.ds(pl.multiple_of(e * depth, 128), depth)]

        def step(c, nothing):
            at = pl.ds(pl.multiple_of(c * tile, tile), tile)
            product = jnp.dot(columns, qkv[e, :, at], preferred_element_type=jnp.float32)
            summed[:, at] = product if begin else summed[:, at] + product
            return nothing

        lax.fori_loop(0, qkv.shape[2] // tile, step, 0)

    project(d, True)
    one.take_partner()
    project(one.partner, False)
    one.share()
    for copy in inward[3:]:
        copy.wait()
    two.cross()
    two.to_partner()
    one.collect()
    for t in one.mirrors:
        project(one.source(t), False)
        project(one.finish(t), False)

    width = heads * HEAD
    across = n * pairs * HEAD // width_k
    for j in range(n):
        send[j, :, :width] = summed[:, j * width : (j + 1) * width].astype(jnp.bfloat16)
        at = width_q + (j // across) * pairs * HEAD
        send[j, :, width : width + pairs * HEAD] = summed[:, at : at + pairs * HEAD].astype(jnp.bfloat16)
        at = at + width_k
        send[j, :, width + pairs * HEAD :] = summed[:, at : at + pairs * HEAD].astype(jnp.bfloat16)
    own = pltpu.make_async_copy(send.at[s], got.at[s], local.at[5])
    own.start()
    q_args = lambda j: send.at[j], lambda j: got.at[j], lambda k: q_send.at[k], lambda k: q_recv.at[k]
    q_copies = exchange(*q_args)
    two.share()
    arrive(*gate_args[1:])
    for j in range(n):
        gate_row[:, j * positions : (j + 1) * positions] = gate_got[j]
    gate_column[...] = jnp.transpose(gate_row[...])
    own.wait()
    arrive(*q_args[1:])

    rows = math.gcd(length, 256)
    own_copies, r_copies = [], []
    for q in range(sequences):
        top = q * positions
        for j in range(n):
            part = got[j, top : top + positions, width : width + pairs * HEAD]
            keys[j * positions : (j + 1) * positions, :] = part
            values[j * positions : (j + 1) * positions, :] = got[j, top : top + positions, width + pairs * HEAD :]
        blocks = rows // positions
        for head in range(heads):
            lanes = slice(head * HEAD, (head + 1) * HEAD)
            pair = head * pairs // heads
            kv = slice(pair * HEAD, (pair + 1) * HEAD)
            gate = q * heads + head

            def q_of(start, count):
                return got[pl.ds(start // positions, count // positions), top : top + positions, lanes].reshape(
                    count, HEAD
                )

            def store(block, value):
                att[q, pl.ds(block * blocks, blocks), :, lanes] = value.reshape(blocks, positions, HEAD)

            if length <= 1024:
                for block in range(length // rows):
                    start = block * rows
                    store(block, attend_rows(
                        q_of(start, rows),
                        lambda lo, hi: keys[lo:hi, kv],
                        lambda lo, hi: values[lo:hi, kv],
                        gate_column[start : start + rows, gate : gate + 1],
                        lambda lo, hi: gate_row[gate : gate + 1, lo:hi],
                        start,
                        rows,
                    ))
            else:
                attend_long(
                    q_of,
                    lambda lo, count: keys[pl.ds(lo, count), kv],
                    lambda lo, count: values[pl.ds(lo, count), kv],
                    lambda lo, count: gate_column[pl.ds(lo, count), gate : gate + 1],
                    lambda lo, count: gate_row[gate : gate + 1, pl.ds(lo, count)],
                    store,
                    length,
                    rows,
                )
        copy = pltpu.make_async_copy(att.at[q, s], ret.at[q, s], local.at[6 + q])
        copy.start()
        own_copies.append(copy)
        r_copies += exchange(
            lambda j: att.at[q, j], lambda j: ret.at[q, j], lambda k: r_send.at[q, k], lambda k: r_recv.at[q, k]
        )
        if q == 0:
            two.take_partner()
            two.collect()
    for t in two.mirrors:
        two.finish(t)
    for q in range(sequences):
        own_copies[q].wait()
        arrive(lambda j: ret.at[q, j], lambda k: r_send.at[q, k], lambda k: r_recv.at[q, k])
        for j in range(n):
            lhs[q * positions : (q + 1) * positions, j * width : (j + 1) * width] = ret[q, j]

    depth_out = outw.shape[1]
    tile_out = math.gcd(outw.shape[2], 256)

    def produce(c, nothing):
        at = pl.ds(pl.multiple_of(c * tile_out, tile_out), tile_out)
        total = jnp.dot(lhs[:, :depth_out], outw[0, :, at], preferred_element_type=jnp.float32)
        for e in range(1, m):
            block = lhs[:, e * depth_out : (e + 1) * depth_out]
            total = total + jnp.dot(block, outw[e, :, at], preferred_element_type=jnp.float32)
        out[:, at] = total.astype(jnp.bfloat16)
        return nothing

    lax.fori_loop(0, outw.shape[2] // tile_out, produce, 0)
    one.drain()
    two.drain()
    for copy in gate_copies + q_copies + r_copies:
        copy.wait_send()


def on_device(n, m, hidden_states, cumulative_gate, query_weight, key_weight, value_weight, out_weight):
    sequences, positions, model_width = hidden_states.shape
    count = sequences * positions
    all_heads = cumulative_gate.shape[2]
    heads = all_heads // n
    copies = max(1, n // KV_HEADS)
    pairs = KV_HEADS * copies // n
    length = positions * n
    gates = jnp.transpose(cumulative_gate.reshape(sequences, positions, n, heads), (2, 0, 3, 1))
    gates = gates.reshape(n, sequences * heads, positions)
    lines = -(-sequences * heads // 8) * 8
    gates = jnp.pad(gates, ((0, 0), (0, lines - sequences * heads), (0, 0)))
    width = heads * HEAD
    wide = query_weight.shape[1] + 2 * key_weight.shape[1]
    shard = query_weight.shape[0]
    dma, bf, f32 = pltpu.SemaphoreType.DMA, jnp.bfloat16, jnp.float32
    vmem, anywhere = pl.BlockSpec(memory_space=pltpu.VMEM), pl.BlockSpec(memory_space=pl.ANY)
    mixed = pl.pallas_call(
        functools.partial(layer_kernel, n, m, sequences, heads, pairs),
        out_shape=jax.ShapeDtypeStruct((count, model_width), bf),
        in_specs=[vmem, vmem] + [anywhere] * 4,
        out_specs=vmem,
        scratch_shapes=[
            pltpu.VMEM((m, shard, wide), bf),
            pltpu.VMEM((m, out_weight.shape[0], model_width), bf),
            pltpu.VMEM((count, wide), f32),
            pltpu.VMEM((n, count, width + 2 * pairs * HEAD), bf),
            pltpu.VMEM((n, count, width + 2 * pairs * HEAD), bf),
            pltpu.VMEM((n, lines, positions), f32),
            pltpu.VMEM((lines, length), f32),
            pltpu.VMEM((length, lines), f32),
            pltpu.VMEM((length, pairs * HEAD), bf),
            pltpu.VMEM((length, pairs * HEAD), bf),
            pltpu.VMEM((sequences, n, positions, width), bf),
            pltpu.VMEM((sequences, n, positions, width), bf),
            pltpu.VMEM((count, out_weight.shape[0] * m), bf),
            *gather_sems(n, m),
            *gather_sems(n, m),
            dma((6 + sequences,)),
            dma((n,)),
            dma((n,)),
            dma((n,)),
            dma((n,)),
            dma((sequences, n)),
            dma((sequences, n)),
        ],
        compiler_params=pltpu.CompilerParams(
            collective_id=0, has_side_effects=True, vmem_limit_bytes=60 * 1024 * 1024
        ),
    )(
        hidden_states.reshape(count, model_width), gates, query_weight, key_weight, value_weight, out_weight
    )
    return mixed.reshape(sequences, positions, model_width)


def solution(mesh):
    placed = (
        P("dp", "sp", None),
        P("dp", "sp", None),
        P("dp", None),
        P("dp", None),
        P("dp", None),
        P("dp", None),
    )
    return jax.shard_map(
        functools.partial(on_device, mesh.shape["sp"], mesh.shape["dp"]),
        mesh=mesh, in_specs=placed, out_specs=P("dp", "sp", None), check_vma=False,
    )
```

time: 216 us -> 183 us (0.85)
  Pallas kernels: 16 us -> 176 us
  waiting for transfers between devices: 112 us -> 0 us
  blocking collectives: 29.4 us -> 0 us
  matrix products: 15 us -> 0 us
  between operations: 13.5 us -> 0.01 us
  starting transfers between devices: 11.3 us -> 0 us
  other arithmetic: 6.15 us -> 0 us
  local copies, waits for them, and re-layouts: 8.16 us -> 3.68 us
    pallas_call x1, Pallas kernels: 16 us -> 176 us  [on_device(): pl.pallas_call(functools.partial(layer_kernel, n, m, sequences, heads, pa...]
    all_gather x2 -> x0, waiting for transfers between devices: 76.7 us -> none  [the longest x1 76.7 us: on_device(): joined = lax.all_gather(joined, 'dp', axis=0, tiled=True)]
    all_to_all x2 -> x0, waiting for transfers between devices: 34.9 us -> none  [the longest x1 34.9 us: on_device(): got = lax.all_to_all(sent, 'sp', split_axis=2, concat_axis=1, tiled=True)]
    all_to_all x1 -> x0, blocking collectives: 29.4 us -> none  [on_device(): lax.all_to_all(attended, 'sp', split_axis=1, concat_axis=2, tiled=True)]
    dot_general x2 -> x0, matrix products: 15 us -> none  [the longest x1 8.3 us: on_device(): jnp.dot(token_rows, joined, preferred_element_type=jnp.float32)]
    all_to_all x2 -> x0, starting transfers between devices: 11.2 us -> none  [the longest x1 5.72 us: on_device(): lax.all_to_all(cumulative_gate, 'sp', split_axis=2, concat_axis=1, tiled=...]
    concatenate x2 -> x0, other arithmetic: 6.15 us -> none  [the longest x1 3.29 us: on_device(): joined = jnp.concatenate([query_weight, key_weight, value_weight], axis=1)]
    all_to_all x5 -> x0, local copies, waits for them, and re-layouts: 2.58 us -> none  [the longest x1 1.61 us: on_device(): got = lax.all_to_all(sent, 'sp', split_axis=2, concat_axis=1, tiled=True)]
  transfers between devices with their start and end apart: 4 -> 0, of which waited for: 2 -> 0; matrix products, arithmetic and copies ran while one was open for 9% -> 0% of each run, Pallas kernels for 8% -> 0%
where the time goes in v2:
time: 183 us; the launch traced here: 180 us
  Pallas kernels  176 us (96%)
  local copies, waits for them, and re-layouts  3.68 us (2%)
    pallas_call x1, Pallas kernels, on_device(): pl.pallas_call(functools.partial(layer_kernel, n, m, sequences, heads, pa...  176 us

profile of v2, /device:TPU:9, one launch (start us, length us, event | category | flops | bytes accessed | tf_op | source)
XLA Modules:
  0.0 180.1 jit_solution(4555656265157606775)
XLA Ops:
  0.0 1.4 copy.7
  1.4 176.4 %shard_map.64 = bf16[256,2048]{1,0:T(8,128)(2,1)} custom-call(bf16[256,2048]{1,0:T(8,128)(2,1)} %bitcast.7, f32[8,8,128]{2,1,0:T(8,128)} %bitcast.8, bf16[512,2048]{1,0:T(8,128)(2,1)} %wq.1, bf16[512,512]{1,0:T(8,128)(2,1)} %wk.1, bf16[512,512]{1,0:T(8,128)(2,1)} %wv.1, bf16[512,2048]{1,0:T(8,128)(2,1)} %wo.1), custom_call_target="tpu_custom_call" | custom-call | tf_op jit(solution)/shard_map/pallas_call | solution.py:389
  177.8 2.3 %copy.9 = bf16[2,128,2048]{2,1,0:T(8,128)(2,1)} copy(bf16[2,128,2048]{2,1,0:T(8,128)(2,1)} %bitcast.6) | data formatting | bytes 2097152

commit v3 on v2

--- a/solution.py
+++ b/solution.py
@@ -10,6 +10,7 @@
 
 KV_HEADS = 8
 HEAD = 64
+SHARE_KV, SHARE_Q, SHARE_OUT = 3, 2, 0
 
 
 def attend_rows(q, k_of, v_of, gate_column, gate_row_of, start, rows):
@@ -75,14 +76,14 @@
 
 
 class Gather:
-    def __init__(self, buf, n, m, me, sems):
+    def __init__(self, buf, n, m, me, sems, eighths):
         self.buf, self.n, self.m = buf, n, m
         self.s, self.d = me
         self.have, self.partner_have, self.own_recv, self.send_a, self.send_b, self.send_c, self.own_send = sems
         self.partner = self.d + 1 - 2 * lax.rem(self.d, 2)
         self.y, self.z = lax.rem(self.s, 2), self.s // 2
         self.big = n // 2
-        self.r1, self.r2 = split_rows(buf.shape[1], n)
+        self.r1, self.r2 = split_rows(buf.shape[1], n, eighths)
         self.started = []
         self.mirrors = range(1, m // 2)
 
@@ -173,9 +174,9 @@
             copy.wait_send()
 
 
-def split_rows(rows, n):
+def split_rows(rows, n, eighths):
     big = n // 2
-    many = rows * 5 // 8 // big // 16 * 16
+    many = rows * eighths // 8 // big // 16 * 16
     return (rows - many * big) // 2, many
 
 
@@ -186,21 +187,21 @@
 
 
 def layer_kernel(n, m, sequences, heads, pairs, hidden, gates, wq, wk, wv, wo, out,
-                 qkv, outw, summed, send, got, gate_got, gate_row, gate_column, keys, values, att, ret, lhs, *sems):
+                 kvw, qw, outw, summed_kv, summed_q, send_kv, got_kv, send, got, gate_got, gate_row, gate_column, keys, values, att, ret, lhs, *sems):
     s, d = lax.axis_index("sp"), lax.axis_index("dp")
-    first, second = sems[:7], sems[7:14]
-    local, gate_send, gate_recv, q_send, q_recv, r_send, r_recv = sems[14:]
+    local, gate_send, gate_recv, kv_send, kv_recv, q_send, q_recv, r_send, r_recv = sems[21:]
     positions = hidden.shape[0] // sequences
     length = positions * n
     mesh_id = pl.DeviceIdType.MESH
-    one = Gather(qkv, n, m, (s, d), first)
-    two = Gather(outw, n, m, (s, d), second)
-    width_q, width_k = wq.shape[1], wk.shape[1]
+    zero = Gather(kvw, n, m, (s, d), sems[:7], SHARE_KV)
+    one = Gather(qw, n, m, (s, d), sems[7:14], SHARE_Q)
+    two = Gather(outw, n, m, (s, d), sems[14:21], SHARE_OUT)
+    width_k = wk.shape[1]
 
     inward = [
-        pltpu.make_async_copy(wq, qkv.at[d, :, pl.ds(0, width_q)], local.at[0]),
-        pltpu.make_async_copy(wk, qkv.at[d, :, pl.ds(width_q, width_k)], local.at[1]),
-        pltpu.make_async_copy(wv, qkv.at[d, :, pl.ds(width_q + width_k, width_k)], local.at[2]),
+        pltpu.make_async_copy(wk, kvw.at[d, :, pl.ds(0, width_k)], local.at[0]),
+        pltpu.make_async_copy(wv, kvw.at[d, :, pl.ds(width_k, width_k)], local.at[1]),
+        pltpu.make_async_copy(wq, qw.at[d], local.at[2]),
         pltpu.make_async_copy(wo, outw.at[d], local.at[3]),
         pltpu.make_async_copy(gates.at[s], gate_got.at[s], local.at[4]),
     ]
@@ -233,68 +234,99 @@
                 device_id=(lax.rem(s + k, n), d), device_id_type=mesh_id,
             ).wait_recv()
 
-    for copy in inward[:3]:
-        copy.wait()
+    inward[0].wait()
+    inward[1].wait()
+    zero.cross()
+    zero.to_partner()
+    inward[2].wait()
     one.cross()
     one.to_partner()
+    inward[4].wait()
     gate_args = lambda j: gates.at[j], lambda j: gate_got.at[j], lambda k: gate_send.at[k], lambda k: gate_recv.at[k]
     gate_copies = exchange(*gate_args)
-
-    depth = qkv.shape[1]
-    tile = math.gcd(qkv.shape[2], 512)
-
-    def project(e, begin):
+    inward[3].wait()
+    two.cross()
+
+    depth = qw.shape[1]
+
+    def project(weight, summed, e, begin):
+        tile = math.gcd(weight.shape[2], 512)
         columns = hidden[:, pl.ds(pl.multiple_of(e * depth, 128), depth)]
 
         def step(c, nothing):
             at = pl.ds(pl.multiple_of(c * tile, tile), tile)
-            product = jnp.dot(columns, qkv[e, :, at], preferred_element_type=jnp.float32)
+            product = jnp.dot(columns, weight[e, :, at], preferred_element_type=jnp.float32)
             summed[:, at] = product if begin else summed[:, at] + product
             return nothing
 
-        lax.fori_loop(0, qkv.shape[2] // tile, step, 0)
-
-    project(d, True)
+        lax.fori_loop(0, weight.shape[2] // tile, step, 0)
+
+    project(kvw, summed_kv, d, True)
+    zero.take_partner()
+    project(kvw, summed_kv, zero.partner, False)
+    project(qw, summed_q, d, True)
+    zero.share()
+    zero.collect()
+    for t in zero.mirrors:
+        project(kvw, summed_kv, zero.source(t), False)
+        project(kvw, summed_kv, zero.finish(t), False)
+
+    width, thin = heads * HEAD, pairs * HEAD
+    across = n * thin // width_k
+    for j in range(n):
+        at = (j // across) * thin
+        send_kv[j, :, :thin] = summed_kv[:, at : at + thin].astype(jnp.bfloat16)
+        send_kv[j, :, thin:] = summed_kv[:, width_k + at : width_k + at + thin].astype(jnp.bfloat16)
+    own_kv = pltpu.make_async_copy(send_kv.at[s], got_kv.at[s], local.at[5])
+    own_kv.start()
+    kv_args = lambda j: send_kv.at[j], lambda j: got_kv.at[j], lambda k: kv_send.at[k], lambda k: kv_recv.at[k]
+    kv_copies = exchange(*kv_args)
+
     one.take_partner()
-    project(one.partner, False)
+    project(qw, summed_q, one.partner, False)
     one.share()
-    for copy in inward[3:]:
-        copy.wait()
-    two.cross()
     two.to_partner()
     one.collect()
     for t in one.mirrors:
-        project(one.source(t), False)
-        project(one.finish(t), False)
-
-    width = heads * HEAD
-    across = n * pairs * HEAD // width_k
-    for j in range(n):
-        send[j, :, :width] = summed[:, j * width : (j + 1) * width].astype(jnp.bfloat16)
-        at = width_q + (j // across) * pairs * HEAD
-        send[j, :, width : width + pairs * HEAD] = summed[:, at : at + pairs * HEAD].astype(jnp.bfloat16)
-        at = at + width_k
-        send[j, :, width + pairs * HEAD :] = summed[:, at : at + pairs * HEAD].astype(jnp.bfloat16)
-    own = pltpu.make_async_copy(send.at[s], got.at[s], local.at[5])
-    own.start()
-    q_args = lambda j: send.at[j], lambda j: got.at[j], lambda k: q_send.at[k], lambda k: q_recv.at[k]
-    q_copies = exchange(*q_args)
-    two.share()
+        project(qw, summed_q, one.source(t), False)
+        project(qw, summed_q, one.finish(t), False)
+    q_copies, own_q = [], []
+
+    def q_args(q):
+        part = pl.ds(q * positions, positions)
+        return (
+            lambda j: send.at[j, part],
+            lambda j: got.at[j, part],
+            lambda k: q_send.at[q, k],
+            lambda k: q_recv.at[q, k],
+        )
+
+    for q in range(sequences):
+        lines = slice(q * positions, (q + 1) * positions)
+        for j in range(n):
+            send[j, lines, :] = summed_q[lines, j * width : (j + 1) * width].astype(jnp.bfloat16)
+        copy = pltpu.make_async_copy(q_args(q)[0](s), q_args(q)[1](s), local.at[6 + q])
+        copy.start()
+        own_q.append(copy)
+        q_copies += exchange(*q_args(q))
     arrive(*gate_args[1:])
     for j in range(n):
         gate_row[:, j * positions : (j + 1) * positions] = gate_got[j]
     gate_column[...] = jnp.transpose(gate_row[...])
-    own.wait()
-    arrive(*q_args[1:])
+    own_kv.wait()
+    arrive(*kv_args[1:])
 
     rows = math.gcd(length, 256)
     own_copies, r_copies = [], []
     for q in range(sequences):
         top = q * positions
         for j in range(n):
-            part = got[j, top : top + positions, width : width + pairs * HEAD]
-            keys[j * positions : (j + 1) * positions, :] = part
-            values[j * positions : (j + 1) * positions, :] = got[j, top : top + positions, width + pairs * HEAD :]
+            keys[j * positions : (j + 1) * positions, :] = got_kv[j, top : top + positions, :thin]
+            values[j * positions : (j + 1) * positions, :] = got_kv[j, top : top + positions, thin:]
+        own_q[q].wait()
+        arrive(*q_args(q)[1:])
+        if q == 0:
+            two.share()
         blocks = rows // positions
         for head in range(heads):
             lanes = slice(head * HEAD, (head + 1) * HEAD)
@@ -333,15 +365,14 @@
                     length,
                     rows,
                 )
-        copy = pltpu.make_async_copy(att.at[q, s], ret.at[q, s], local.at[6 + q])
+        copy = pltpu.make_async_copy(att.at[q, s], ret.at[q, s], local.at[6 + sequences + q])
         copy.start()
         own_copies.append(copy)
         r_copies += exchange(
             lambda j: att.at[q, j], lambda j: ret.at[q, j], lambda k: r_send.at[q, k], lambda k: r_recv.at[q, k]
         )
-        if q == 0:
-            two.take_partner()
-            two.collect()
+    two.take_partner()
+    two.collect()
     for t in two.mirrors:
         two.finish(t)
     for q in range(sequences):
@@ -363,9 +394,10 @@
         return nothing
 
     lax.fori_loop(0, outw.shape[2] // tile_out, produce, 0)
+    zero.drain()
     one.drain()
     two.drain()
-    for copy in gate_copies + q_copies + r_copies:
+    for copy in gate_copies + kv_copies + q_copies + r_copies:
         copy.wait_send()
 
 
@@ -382,7 +414,7 @@
     lines = -(-sequences * heads // 8) * 8
     gates = jnp.pad(gates, ((0, 0), (0, lines - sequences * heads), (0, 0)))
     width = heads * HEAD
-    wide = query_weight.shape[1] + 2 * key_weight.shape[1]
+    wide, narrow = query_weight.shape[1], 2 * key_weight.shape[1]
     shard = query_weight.shape[0]
     dma, bf, f32 = pltpu.SemaphoreType.DMA, jnp.bfloat16, jnp.float32
     vmem, anywhere = pl.BlockSpec(memory_space=pltpu.VMEM), pl.BlockSpec(memory_space=pl.ANY)
@@ -392,11 +424,15 @@
         in_specs=[vmem, vmem] + [anywhere] * 4,
         out_specs=vmem,
         scratch_shapes=[
+            pltpu.VMEM((m, shard, narrow), bf),
             pltpu.VMEM((m, shard, wide), bf),
             pltpu.VMEM((m, out_weight.shape[0], model_width), bf),
+            pltpu.VMEM((count, narrow), f32),
             pltpu.VMEM((count, wide), f32),
-            pltpu.VMEM((n, count, width + 2 * pairs * HEAD), bf),
-            pltpu.VMEM((n, count, width + 2 * pairs * HEAD), bf),
+            pltpu.VMEM((n, count, 2 * pairs * HEAD), bf),
+            pltpu.VMEM((n, count, 2 * pairs * HEAD), bf),
+            pltpu.VMEM((n, count, width), bf),
+            pltpu.VMEM((n, count, width), bf),
             pltpu.VMEM((n, lines, positions), f32),
             pltpu.VMEM((lines, length), f32),
             pltpu.VMEM((length, lines), f32),
@@ -407,11 +443,14 @@
             pltpu.VMEM((count, out_weight.shape[0] * m), bf),
             *gather_sems(n, m),
             *gather_sems(n, m),
-            dma((6 + sequences,)),
+            *gather_sems(n, m),
+            dma((6 + 2 * sequences,)),
             dma((n,)),
             dma((n,)),
             dma((n,)),
             dma((n,)),
+            dma((sequences, n)),
+            dma((sequences, n)),
             dma((sequences, n)),
             dma((sequences, n)),
         ],

time: 183 us -> 124 us (0.68); the launches traced: 180 us -> 123 us
  Pallas kernels: 176 us -> 120 us
    pallas_call x1, Pallas kernels: 176 us -> 120 us  [on_device(): pl.pallas_call(functools.partial(layer_kernel, n, m, sequences, heads, pa...]
where the time goes in v3:
time: 124 us; the launch traced here: 123 us
  Pallas kernels  120 us (97%)
  local copies, waits for them, and re-layouts  3.68 us (3%)
    pallas_call x1, Pallas kernels, on_device(): pl.pallas_call(functools.partial(layer_kernel, n, m, sequences, heads, pa...  120 us

profile of v3, /device:TPU:9, one launch (start us, length us, event | category | flops | bytes accessed | tf_op | source)
XLA Modules:
  0.0 123.3 jit_solution(7643837148007221430)
XLA Ops:
  0.0 1.4 %copy.7 = f32[2,128,8,4]{1,3,0,2:T(4,128)} copy(f32[2,128,8,4]{1,3,2,0:T(4,128)} %bitcast.9) | data formatting | bytes 65536 | tf_op jit(solution)/shard_map/reshape | solution.py:412
  1.4 119.7 %shard_map.64 = bf16[256,2048]{1,0:T(8,128)(2,1)} custom-call(bf16[256,2048]{1,0:T(8,128)(2,1)} %bitcast.7, f32[8,8,128]{2,1,0:T(8,128)} %bitcast.8, bf16[512,2048]{1,0:T(8,128)(2,1)} %wq.1, bf16[512,512]{1,0:T(8,128)(2,1)} %wk.1, bf16[512,512]{1,0:T(8,128)(2,1)} %wv.1, bf16[512,2048]{1,0:T(8,128)(2,1)} %wo.1), custom_call_target="tpu_custom_call" | custom-call | tf_op jit(solution)/shard_map/pallas_call | solution.py:421
  121.0 2.3 %copy.9 = bf16[2,128,2048]{2,1,0:T(8,128)(2,1)} copy(bf16[2,128,2048]{2,1,0:T(8,128)(2,1)} %bitcast.6) | data formatting | bytes 2097152
